TPU v7x, 512 devices: a whole 4x4x16 slice. The times are simulated.
512 devices in a mesh: sp: 32 (over z, core), tp: 16 (over y, x).
Axes of the slice: x: 4, y: 4, z: 16, core: 2. Of those that a mesh axis runs over, the one named last changes fastest.
Arguments:
- residual_in: bfloat16 [8192, 2048], P('sp'), may hold values from -3 to 3
- mix_gain: float32 [2048], replicated, may hold values from 0.1 to 1.9
- pool_weight: bfloat16 [512, 2048], P(None, 'tp'), may hold values from -0.5 to 0.5
- pool_scale: float32 [2048], P('tp'), may hold values from 0.1 to 1.9
- ffn_gain: float32 [2048], replicated, may hold values from 0.1 to 1.9
- route_ids: int32 [8192, 2], P('sp'), may hold values from 0 to 31, all different within a row; in each aligned block of 16 rows (0 to 15, 16 to 31, ...) at most 2 rows name the same one
- route_weights: float32 [8192, 2], P('sp'), may hold values from 0.1 to 1
- gate_weight: bfloat16 [32, 2048, 3584], P('sp', None, 'tp'), may hold values from -0.125 to 0.125
- up_weight: bfloat16 [32, 2048, 3584], P('sp', None, 'tp'), may hold values from -0.125 to 0.125
- down_weight: bfloat16 [32, 3584, 2048], P('sp', 'tp'), may hold values from -0.09375 to 0.09375
Outputs:
- layer_out: bfloat16 [8192, 2048], P('sp')
Inputs may be any that keep to these rules, and one draw needn't show every extreme that they name: `route_ids`: each row names 2 different experts; in each aligned block of 16 rows no expert is named by more than 2 rows, and some block has an expert named by exactly 2 rows.
All inputs are finite; a program needn't handle non-finite values.
Results may differ from a plain program's by a relative error of at most 0.0074.
Values may be sent and summed in bfloat16 or wider, within the bound.
No kernel may reach another device: no remote copies, remote signals or barrier semaphores. Data moves between devices by JAX's collectives and lax.ppermute only.
A program may use at most 64 MiB of HBM per device.

v0:
```python
import jax
import jax.numpy as jnp
from jax import lax
from jax.sharding import Mesh
from jax.sharding import PartitionSpec as P

GROUPS = 4
SPAN = 16
TOP_K = 2
SP = ("sp_0", "sp_1")
EPS = 1e-06


def from_behind(value, axis, steps):
    count = lax.axis_size(axis)
    first, last = (max(0, -steps), min(count, count - steps))
    return lax.ppermute(value, axis, [(source, source + steps) for source in range(first, last)])


def split_up(shard, dim, size):
    before, after = (shard.shape[:dim], shard.shape[dim + 1 :])
    return jnp.moveaxis(shard.reshape(*before, size, -1, *after), dim, 0)


def sent_and_summed(shard, axis, dim):
    size = lax.axis_size(axis)
    blocks = lax.all_to_all(split_up(shard, dim, size), axis, 0, 0, tiled=True)
    return jnp.sum(blocks.astype(jnp.float32), axis=0)


def in_order(blocks, dim):
    dims = list(blocks.shape[1:])
    dims[dim] *= blocks.shape[0]
    return jnp.moveaxis(blocks, 0, dim).reshape(dims)


def exchange_in_order(blocks, axes, order):
    dims = [lax.axis_size(a) for a in axes]
    blocks = blocks.reshape(*dims, *blocks.shape[1:])
    for k in order:
        blocks = lax.all_to_all(blocks, axes[k], split_axis=k, concat_axis=k, tiled=True)
    return blocks.reshape(-1, *blocks.shape[len(axes) :])


def core_and_chips(shard, groups, order, split_dim, concat_dim):
    size = lax.axis_size(groups[0]) * lax.axis_size(groups[1])
    blocks = split_up(shard, split_dim, size)
    return in_order(exchange_in_order(blocks, groups, order), concat_dim)


def copy_for_each(shard, axis):
    size = lax.axis_size(axis)
    return lax.all_to_all(
        jnp.broadcast_to(shard[None], (size, *shard.shape)), axis, 0, 0, tiled=True
    )


def gather_directly(shard, axis, dim):
    blocks = copy_for_each(shard, axis)
    return in_order(blocks, dim)


def rms_scale(values, gain):
    return values * lax.rsqrt(jnp.mean(values * values, axis=-1, keepdims=True) + EPS) * gain


def slot_table(chosen_ids, experts, capacity):
    flat_ids = chosen_ids.reshape(-1)
    matches = (flat_ids[:, None] == jnp.arange(experts, dtype=jnp.int32)[None, :]).astype(jnp.int32)
    before = jnp.cumsum(matches, axis=0) - matches
    slot_of = jnp.sum(before * matches, axis=1)
    target = flat_ids * capacity + slot_of
    return (target[:, None] == jnp.arange(experts * capacity, dtype=jnp.int32)[None, :]).astype(
        jnp.float32
    )


def shards(
    residual_in,
    mix_gain,
    pool_weight,
    pool_scale,
    ffn_gain,
    route_ids,
    route_weights,
    gate_weight,
    up_weight,
    down_weight,
):
    tp_count = lax.axis_size("tp")
    sp_count = lax.axis_size(SP)
    tp_index = lax.axis_index("tp")
    tok_count, width = residual_in.shape
    group_width = width // GROUPS
    col_count = pool_weight.shape[1]
    row_count = tok_count // tp_count
    capacity = 2 * TOP_K * row_count // sp_count
    group_index = tp_index * col_count // group_width
    window = jnp.power(2, group_index + 1)
    stream = residual_in.astype(jnp.float32)
    inverse = lax.rsqrt(jnp.mean(stream * stream, axis=-1, keepdims=True) + EPS)
    stream_group = lax.dynamic_slice_in_dim(stream, group_index * group_width, group_width, 1)
    gain_group = lax.dynamic_slice_in_dim(mix_gain, group_index * group_width, group_width, 0)
    normed_group = (stream_group * inverse * gain_group).astype(jnp.bfloat16)
    rim_rows = from_behind(normed_group[tok_count - SPAN :], SP, 1)
    extended = jnp.concatenate([rim_rows, normed_group], axis=0).astype(jnp.float32)
    window_sum = jnp.zeros((tok_count, group_width), jnp.float32)
    for offset in range(SPAN):
        window_sum = window_sum + jnp.where(
            offset < window, extended[SPAN - offset : SPAN - offset + tok_count], 0.0
        )
    position = lax.axis_index(SP) * tok_count + jnp.arange(tok_count, dtype=jnp.int32)
    divisor = jnp.minimum(position + 1, window).astype(jnp.float32)
    pooled = (window_sum / divisor[:, None] - extended[SPAN:]).astype(jnp.bfloat16)
    mixed = (jnp.dot(pooled, pool_weight, preferred_element_type=jnp.float32) * pool_scale).astype(
        jnp.bfloat16
    )
    stream_own = lax.dynamic_slice_in_dim(stream, tp_index * row_count, row_count, 0)
    mixed_own = lax.all_to_all(mixed, "tp", split_axis=0, concat_axis=1, tiled=True)
    after_own = (stream_own + mixed_own.astype(jnp.float32)).astype(jnp.bfloat16)
    normed_own = rms_scale(after_own.astype(jnp.float32), ffn_gain).astype(jnp.bfloat16)
    ids_own = lax.dynamic_slice_in_dim(route_ids, tp_index * row_count, row_count, 0)
    table_own = slot_table(ids_own, sp_count, capacity)
    repeated = jnp.repeat(normed_own, TOP_K, axis=0)
    outgoing = lax.dot_general(
        table_own.astype(jnp.bfloat16),
        repeated,
        (((0,), (0,)), ((), ())),
        preferred_element_type=jnp.float32,
    )
    outgoing = outgoing.astype(jnp.bfloat16).reshape(sp_count, capacity, width)
    arrived = lax.all_to_all(outgoing, SP, split_axis=0, concat_axis=0, tiled=True)
    piece = lax.all_gather(arrived, "tp", axis=0, tiled=True)
    flat_rows = piece.reshape(-1, width)
    gate_part = jnp.dot(flat_rows, gate_weight[0], preferred_element_type=jnp.float32)
    up_part = jnp.dot(flat_rows, up_weight[0], preferred_element_type=jnp.float32)
    hidden = (jax.nn.silu(gate_part) * up_part).astype(jnp.bfloat16)
    hidden_all = hidden.reshape(piece.shape[0], piece.shape[1], hidden.shape[1])
    hidden_flat = hidden_all.reshape(-1, hidden_all.shape[-1])
    term = jnp.dot(hidden_flat, down_weight[0], preferred_element_type=jnp.float32)
    summed = sent_and_summed(
        term.astype(jnp.bfloat16).astype(jnp.float32).astype(jnp.bfloat16), "tp", 0
    )
    expert_out = summed.astype(jnp.bfloat16).reshape(sp_count, capacity, width)
    returned_rows = core_and_chips(expert_out, ("sp_0", "sp_1"), (1, 0), 0, 0)
    weights_own = lax.dynamic_slice_in_dim(route_weights, tp_index * row_count, row_count, 0)
    weight_table = jnp.einsum(
        "rk,rkc->rc", weights_own, table_own.reshape(row_count, TOP_K, sp_count * capacity)
    )
    expert_mix = jnp.dot(
        weight_table,
        returned_rows.reshape(-1, width).astype(jnp.float32),
        precision=lax.Precision.HIGHEST,
    )
    out_own = (after_own.astype(jnp.float32) + expert_mix).astype(jnp.bfloat16)
    return gather_directly(out_own, "tp", 0)


def solution(mesh):
    torus = Mesh(mesh.devices.reshape(16, 2, mesh.shape["tp"]), ("sp_0", "sp_1", "tp"))
    return jax.shard_map(
        shards,
        mesh=torus,
        in_specs=(
            P(SP, None),
            P(),
            P(None, "tp"),
            P("tp"),
            P(),
            P(SP, None),
            P(SP, None),
            P(SP, None, "tp"),
            P(SP, None, "tp"),
            P(SP, "tp", None),
        ),
        out_specs=P(SP, None),
        check_vma=False,
    )
```

profile of v0, /device:TPU:32, one launch (start us, length us, event | category | flops | bytes accessed | tf_op | source)
XLA Modules:
  0.0 268.7 jit_solution(1426922073096499499)
XLA Ops:
  6.5 1.6 multiply_reduce_fusion
  8.1 1.5 convert_element_type.67
  9.6 0.8 dynamic_slice.17
  10.5 1.9 collective-permute-start
  13.1 2.5 collective-permute-done
  15.7 2.0 fusion.2
  17.7 7.0 %all-to-all-start = ((bf16[16,16,128]{2,1,0:T(8,128)(2,1)}), bf16[16,16,128]{2,1,0:T(8,128)(2,1)S(1)}, u32[]{:S(2)}, u32[]{:S(2)}) async-start(bf16[16,16,128]{2,1,0:T(8,128)(2,1)} %bitcast), calls=%async_computation | async-start | bytes 131072 | tf_op jit(solution)/shard_map/all_to_all | solution.py:119
  24.8 7.6 %all-to-all-done = bf16[16,16,128]{2,1,0:T(8,128)(2,1)S(1)} async-done(((bf16[16,16,128]{2,1,0:T(8,128)(2,1)}), bf16[16,16,128]{2,1,0:T(8,128)(2,1)S(1)}, u32[]{:S(2)}, u32[]{:S(2)}) %all-to-all-start) | async-done | bytes 65568 | tf_op jit(solution)/shard_map/all_to_all | solution.py:119
  32.8 0.3 convolution_convert_fusion.1
  33.3 37.4 %all_to_all.38 = bf16[32,2,2048]{2,1,0:T(2,128)(2,1)} all-to-all(bf16[32,2,2048]{2,1,0:T(2,128)(2,1)S(1)} %reshape.68), channel_id=1, replica_groups=mesh['sp_0'=16,'sp_1'=2,'tp'=16] {'sp_0','sp_1'}, dimensions={0} | all-to-all | bytes 524288 | tf_op jit(solution)/shard_map/all_to_all | solution.py:132
  70.8 56.0 %all-gather.2.cloned.1.call-done = bf16[512,2,2048]{2,1,0:T(2,128)(2,1)} async-done(((bf16[32,2,2048]{2,1,0:T(2,128)(2,1)}), bf16[512,2,2048]{2,1,0:T(2,128)(2,1)}) %all-gather.2.cloned.1.call-update) | async-done | bytes 4194320 | tf_op jit(solution)/shard_map/all_gather | solution.py:133
  126.8 7.2 %reshape.69 = bf16[1024,2048]{1,0:T(8,128)(2,1)} reshape(bf16[512,2,2048]{2,1,0:T(2,128)(2,1)} %all-gather.2.cloned.1.call-done) | data formatting | bytes 8388608 | tf_op jit(solution)/shard_map/reshape | solution.py:134
  134.0 4.6 %fusion.6 = f32[1024,224]{0,1:T(8,128)} fusion(bf16[1024,2048]{1,0:T(8,128)(2,1)} %reshape.69, bf16[1,2048,224]{1,2,0:T(8,128)(2,1)S(1)} %copy-done.3), kind=kOutput, calls=%fused_computation.11 | convolution fusion | flops 939524096 | bytes 6029312 | tf_op jit(solution)/shard_map/dot_general | solution.py:135
  138.6 7.0 %convolution_convert_fusion = bf16[1024,2048]{1,0:T(8,128)(2,1)} fusion(bf16[1024,2048]{1,0:T(8,128)(2,1)} %reshape.69, bf16[1,224,2048]{2,1,0:T(8,128)(2,1)S(1)} %copy-done, bf16[1,2048,224]{1,2,0:T(8,128)(2,1)S(1)} %copy-done.4, f32[1024,224]{0,1:T(8,128)} %fusion.6), kind=kOutput, calls=%fused_computation | convolution fusion | flops 1882521600 | bytes 11141120 | tf_op jit(solution)/shard_map/dot_general | solution.py:140
  145.6 56.0 %all_to_all.39 = bf16[16,64,2048]{2,1,0:T(8,128)(2,1)} all-to-all(bf16[16,64,2048]{2,1,0:T(8,128)(2,1)} %bitcast.35), channel_id=1, replica_groups=mesh['sp_0'=16,'sp_1'=2,'tp'=16] {'tp'}, dimensions={0} | all-to-all | bytes 8388608 | tf_op jit(solution)/shard_map/all_to_all | solution.py:27
  201.7 3.0 %reduce_sum.45 = bf16[64,2048]{1,0:T(8,128)(2,1)S(1)} reduce(bf16[16,64,2048]{2,1,0:T(8,128)(2,1)} %all_to_all.39, bf16[]{:T(256)} %constant.97.clone.1), dimensions={0}, to_apply=%region_4.5 | reduce | flops 1966080 | bytes 4456450 | tf_op jit(solution)/shard_map/reduce_sum | solution.py:28
  205.0 3.9 %all_to_all.40 = bf16[16,2,1,2,2048]{4,3,0,2,1:T(2,128)(2,1)S(1)} all-to-all(bf16[16,2,1,2,2048]{4,3,0,2,1:T(2,128)(2,1)S(1)} %copy.20), channel_id=1, replica_groups=mesh['sp_0'=16,'sp_1'=2,'tp'=16] {'sp_1'}, dimensions={1} | all-to-all | bytes 524288 | tf_op jit(solution)/shard_map/all_to_all | solution.py:41
  209.0 1.0 copy.21
  209.9 12.7 %all-to-all-start.4 = ((bf16[16,2,1,2,2048]{4,3,1,2,0:T(2,128)(2,1)}), bf16[16,2,1,2,2048]{4,3,1,2,0:T(2,128)(2,1)S(1)}, u32[]{:S(2)}, u32[]{:S(2)}) async-start(bf16[16,2,1,2,2048]{4,3,1,2,0:T(2,128)(2,1)} %copy.21), calls=%async_computation.4 | async-start | bytes 524288 | tf_op jit(solution)/shard_map/all_to_all | solution.py:41
  222.7 0.8 dynamic-slice_bitcast_fusion
  223.7 17.2 %all-to-all-done.4 = bf16[16,2,1,2,2048]{4,3,1,2,0:T(2,128)(2,1)S(1)} async-done(((bf16[16,2,1,2,2048]{4,3,1,2,0:T(2,128)(2,1)}), bf16[16,2,1,2,2048]{4,3,1,2,0:T(2,128)(2,1)S(1)}, u32[]{:S(2)}, u32[]{:S(2)}) %all-to-all-start.4) | async-done | bytes 262176 | tf_op jit(solution)/shard_map/all_to_all | solution.py:41
  241.1 0.2 fusion
  241.4 19.5 %all_to_all.41 = bf16[16,16,2048]{2,1,0:T(8,128)(2,1)S(1)} all-to-all(bf16[16,16,2048]{2,1,0:T(8,128)(2,1)S(1)} %broadcast_in_dim.39), channel_id=1, replica_groups=mesh['sp_0'=16,'sp_1'=2,'tp'=16] {'tp'}, dimensions={0} | all-to-all | bytes 2097152 | tf_op jit(solution)/shard_map/all_to_all | solution.py:53
  260.9 1.0 copy.29
  (42 shorter events, 2.3 us)
Async XLA Ops:
  6.5 132.1 %copy-start = (bf16[1,224,2048]{2,1,0:T(8,128)(2,1)S(1)}, bf16[1,224,2048]{2,1,0:T(8,128)(2,1)}, u32[]{:S(2)}) copy-start(bf16[1,224,2048]{2,1,0:T(8,128)(2,1)} %param.19) | copy-start | bytes 2752516
  6.5 6.0 %copy-start.2 = (s32[256,2]{0,1:T(2,128)S(1)}, s32[256,2]{0,1:T(2,128)}, u32[]{:S(2)}) copy-start(s32[256,2]{0,1:T(2,128)} %param.15) | copy-start | bytes 6148
  6.5 9.1 %copy-start.6 = (f32[128]{0:T(128)S(1)}, f32[128]{0:T(128)}, u32[]{:S(2)}) copy-start(f32[128]{0:T(128)} %param.13) | copy-start | bytes 1540
  6.5 9.1 %copy-start.5 = (bf16[512,128]{1,0:T(8,128)(2,1)S(1)}, bf16[512,128]{1,0:T(8,128)(2,1)}, u32[]{:S(2)}) copy-start(bf16[512,128]{1,0:T(8,128)(2,1)} %param.12) | copy-start | bytes 393220
  10.5 5.1 %collective-permute-start = (bf16[16,512]{1,0:T(8,128)(2,1)S(1)}, bf16[16,512]{1,0:T(8,128)(2,1)S(1)}, u32[]{:S(2)}, u32[]{:S(2)}) collective-permute-start(bf16[16,512]{1,0:T(8,128)(2,1)S(1)} %slice.69), channel_id=1, source_target_pairs={{0,16},{16,32},{32,48},{48,64},{64,80},{80,96},{96,112},{112,128},... | collective-permute-start | bytes 49160 | tf_op jit(solution)/shard_map/ppermute | solution.py:17
  15.7 16.9 %copy-start.1 = (f32[2048]{0:T(1024)S(1)}, f32[2048]{0:T(1024)}, u32[]{:S(2)}) copy-start(f32[2048]{0:T(1024)} %param.14) | copy-start | bytes 24580
  17.7 14.7 %all-to-all-start = ((bf16[16,16,128]{2,1,0:T(8,128)(2,1)}), bf16[16,16,128]{2,1,0:T(8,128)(2,1)S(1)}, u32[]{:S(2)}, u32[]{:S(2)}) async-start(bf16[16,16,128]{2,1,0:T(8,128)(2,1)} %bitcast), calls=%async_computation | async-start | bytes 131072 | tf_op jit(solution)/shard_map/all_to_all | solution.py:119
  24.8 102.0 %all-gather.2.cloned.1.call-start = ((), (), s32[]{:S(2)}) async-start(), calls=%async_computation.6 | async-start | bytes 4456448 | tf_op jit(solution)/shard_map/all_gather | solution.py:133
  70.8 63.2 %copy-start.3 = (bf16[1,2048,224]{1,2,0:T(8,128)(2,1)S(1)}, bf16[1,2048,224]{1,2,0:T(8,128)(2,1)}, u32[]{:S(2)}) copy-start(bf16[1,2048,224]{1,2,0:T(8,128)(2,1)} %param.17) | copy-start | bytes 2752516
  134.0 4.6 %copy-start.4 = (bf16[1,2048,224]{1,2,0:T(8,128)(2,1)S(1)}, bf16[1,2048,224]{1,2,0:T(8,128)(2,1)}, u32[]{:S(2)}) copy-start(bf16[1,2048,224]{1,2,0:T(8,128)(2,1)} %param.18) | copy-start | bytes 2752516
  209.9 31.0 %all-to-all-start.4 = ((bf16[16,2,1,2,2048]{4,3,1,2,0:T(2,128)(2,1)}), bf16[16,2,1,2,2048]{4,3,1,2,0:T(2,128)(2,1)S(1)}, u32[]{:S(2)}, u32[]{:S(2)}) async-start(bf16[16,2,1,2,2048]{4,3,1,2,0:T(2,128)(2,1)} %copy.21), calls=%async_computation.4 | async-start | bytes 524288 | tf_op jit(solution)/shard_map/all_to_all | solution.py:41
Sparse Core Ops, SparseCore 0:
  70.9 55.8 all-gather.1
where the time goes:
time: 269 us
  blocking collectives  117 us (43%)
  waiting for transfers between devices  83.3 us (31%)
  starting transfers between devices  21.7 us (8%)
  matrix products  14.4 us (5%)
  between operations  13.7 us (5%)
  local copies, waits for them, and re-layouts  12 us (4%)
  other arithmetic  6.75 us (3%)
    all_to_all x1, blocking collectives, sent_and_summed(): blocks = lax.all_to_all(split_up(shard, dim, size), axis, 0, 0, tiled=True)  56 us
    all_gather x1, waiting for transfers between devices, shards(): piece = lax.all_gather(arrived, 'tp', axis=0, tiled=True)  56 us
    all_to_all x1, blocking collectives, shards(): lax.all_to_all(outgoing, SP, split_axis=0, concat_axis=0, tiled=True)  37.4 us
    all_to_all x1, blocking collectives, copy_for_each(): lax.all_to_all(jnp.broadcast_to(shard[None], (size, *shard.shape)), axis,...  19.5 us
    all_to_all x1, waiting for transfers between devices, exchange_in_order(): lax.all_to_all(blocks, axes[k], split_axis=k, concat_axis=k, tiled=True)  17.2 us
    all_to_all x1, starting transfers between devices, exchange_in_order(): lax.all_to_all(blocks, axes[k], split_axis=k, concat_axis=k, tiled=True)  12.7 us
    all_to_all x1, waiting for transfers between devices, shards(): lax.all_to_all(mixed, 'tp', split_axis=0, concat_axis=1, tiled=True)  7.6 us
    reshape x1, local copies, waits for them, and re-layouts, shards(): flat_rows = piece.reshape(-1, width)  7.21 us
  transfers between devices with their start and end apart: 4, of which 4 were waited for; matrix products, arithmetic and copies ran while one was open for 1% of the time, Pallas kernels for 0%

commit v1 on v0

--- a/solution.py
+++ b/solution.py
@@ -130,7 +130,11 @@
     )
     outgoing = outgoing.astype(jnp.bfloat16).reshape(sp_count, capacity, width)
     arrived = lax.all_to_all(outgoing, SP, split_axis=0, concat_axis=0, tiled=True)
-    piece = lax.all_gather(arrived, "tp", axis=0, tiled=True)
+    block_list = []
+    for _ in range(lax.axis_size("tp")):
+        block_list.append(arrived)
+    reply = jnp.concatenate(block_list, axis=0)
+    piece = lax.all_to_all(reply, axis_name="tp", split_axis=0, concat_axis=0, tiled=True)
     flat_rows = piece.reshape(-1, width)
     gate_part = jnp.dot(flat_rows, gate_weight[0], preferred_element_type=jnp.float32)
     up_part = jnp.dot(flat_rows, up_weight[0], preferred_element_type=jnp.float32)

time: 269 us -> 251 us (0.933)
  waiting for transfers between devices: 83.3 us -> 27.3 us
  blocking collectives: 117 us -> 170 us
  between operations: 13.7 us -> 0.34 us
  starting transfers between devices: 21.7 us -> 15.7 us
  local copies, waits for them, and re-layouts: 12 us -> 15.4 us
    all_gather x1 -> x0, waiting for transfers between devices: 56 us -> none  [shards(): piece = lax.all_gather(arrived, 'tp', axis=0, tiled=True)]
    all_to_all x0 -> x1, blocking collectives: none -> 53.8 us  [shards(): lax.all_to_all(reply, axis_name='tp', split_axis=0, concat_axis=0, tiled=...]
    all_to_all x1, starting transfers between devices: 12.7 us -> 6.77 us  [exchange_in_order(): lax.all_to_all(blocks, axes[k], split_axis=k, concat_axis=k, tiled=True)]
    unnamed x16 -> x31, local copies, waits for them, and re-layouts: 1.09 us -> 4.17 us
  transfers between devices with their start and end apart: 4 -> 3, of which waited for: 4 -> 3; matrix products, arithmetic and copies ran while one was open for 1% -> 1% of each run, Pallas kernels for 0% -> 0%
where the time goes in v1:
time: 251 us; the launch traced here: 250 us
  blocking collectives  170 us (68%)
  waiting for transfers between devices  27.3 us (11%)
  starting transfers between devices  15.7 us (6%)
  local copies, waits for them, and re-layouts  15.4 us (6%)
  matrix products  14.4 us (6%)
  other arithmetic  6.75 us (3%)
    all_to_all x1, blocking collectives, sent_and_summed(): blocks = lax.all_to_all(split_up(shard, dim, size), axis, 0, 0, tiled=True)  55.4 us
    all_to_all x1, blocking collectives, shards(): lax.all_to_all(reply, axis_name='tp', split_axis=0, concat_axis=0, tiled=...  53.8 us
    all_to_all x1, blocking collectives, shards(): lax.all_to_all(outgoing, SP, split_axis=0, concat_axis=0, tiled=True)  37.3 us
    all_to_all x1, blocking collectives, copy_for_each(): lax.all_to_all(jnp.broadcast_to(shard[None], (size, *shard.shape)), axis,...  19.4 us
    all_to_all x1, waiting for transfers between devices, exchange_in_order(): lax.all_to_all(blocks, axes[k], split_axis=k, concat_axis=k, tiled=True)  17.2 us
    all_to_all x1, waiting for transfers between devices, shards(): lax.all_to_all(mixed, 'tp', split_axis=0, concat_axis=1, tiled=True)  7.65 us
    reshape x1, local copies, waits for them, and re-layouts, shards(): flat_rows = piece.reshape(-1, width)  7.29 us
    all_to_all x1, starting transfers between devices, shards(): lax.all_to_all(mixed, 'tp', split_axis=0, concat_axis=1, tiled=True)  7.03 us
  transfers between devices with their start and end apart: 3, of which 3 were waited for; matrix products, arithmetic and copies ran while one was open for 1% of the time, Pallas kernels for 0%

profile of v1, /device:TPU:32, one launch (start us, length us, event | category | flops | bytes accessed | tf_op | source)
XLA Modules:
  0.0 249.9 jit_solution(2664294725532684490)
XLA Ops:
  0.0 1.6 multiply_reduce_fusion
  1.6 1.5 convert_element_type.67
  3.1 0.8 dynamic_slice.17
  4.0 1.9 collective-permute-start
  6.6 2.5 collective-permute-done
  9.2 2.0 fusion.2
  11.2 7.0 %all-to-all-start = ((bf16[16,16,128]{2,1,0:T(8,128)(2,1)}), bf16[16,16,128]{2,1,0:T(8,128)(2,1)S(1)}, u32[]{:S(2)}, u32[]{:S(2)}) async-start(bf16[16,16,128]{2,1,0:T(8,128)(2,1)} %bitcast), calls=%async_computation | async-start | bytes 131072 | tf_op jit(solution)/shard_map/all_to_all | solution.py:119
  18.3 7.7 %all-to-all-done = bf16[16,16,128]{2,1,0:T(8,128)(2,1)S(1)} async-done(((bf16[16,16,128]{2,1,0:T(8,128)(2,1)}), bf16[16,16,128]{2,1,0:T(8,128)(2,1)S(1)}, u32[]{:S(2)}, u32[]{:S(2)}) %all-to-all-start) | async-done | bytes 65568 | tf_op jit(solution)/shard_map/all_to_all | solution.py:119
  26.3 0.3 convolution_convert_fusion.1
  26.8 37.3 %all_to_all.43 = bf16[32,2,2048]{2,1,0:T(2,128)(2,1)S(1)} all-to-all(bf16[32,2,2048]{2,1,0:T(2,128)(2,1)S(1)} %reshape.68), channel_id=1, replica_groups=mesh['sp_0'=16,'sp_1'=2,'tp'=16] {'sp_0','sp_1'}, dimensions={0} | all-to-all | bytes 524288 | tf_op jit(solution)/shard_map/all_to_all | solution.py:132
  67.5 53.8 %all_to_all.44 = bf16[512,2,2048]{2,1,0:T(2,128)(2,1)} all-to-all(bf16[512,2,2048]{2,1,0:T(2,128)(2,1)S(1)} %constant_dynamic-update-slice_fusion), channel_id=1, replica_groups=mesh['sp_0'=16,'sp_1'=2,'tp'=16] {'tp'}, dimensions={0} | all-to-all | bytes 8388608 | tf_op jit(solution)/shard_map/all_to_all | solution.py:137
  121.3 7.3 %reshape.69 = bf16[1024,2048]{1,0:T(8,128)(2,1)} reshape(bf16[512,2,2048]{2,1,0:T(2,128)(2,1)} %all_to_all.44) | data formatting | bytes 8388608 | tf_op jit(solution)/shard_map/reshape | solution.py:138
  128.6 4.6 %fusion.6 = f32[1024,224]{0,1:T(8,128)} fusion(bf16[1024,2048]{1,0:T(8,128)(2,1)} %reshape.69, bf16[1,2048,224]{1,2,0:T(8,128)(2,1)S(1)} %copy-done.3), kind=kOutput, calls=%fused_computation.11 | convolution fusion | flops 939524096 | bytes 6029312 | tf_op jit(solution)/shard_map/dot_general | solution.py:139
  133.2 7.0 %convolution_convert_fusion = bf16[1024,2048]{1,0:T(8,128)(2,1)} fusion(bf16[1024,2048]{1,0:T(8,128)(2,1)} %reshape.69, bf16[1,224,2048]{2,1,0:T(8,128)(2,1)S(1)} %copy-done, bf16[1,2048,224]{1,2,0:T(8,128)(2,1)S(1)} %copy-done.4, f32[1024,224]{0,1:T(8,128)} %fusion.6), kind=kOutput, calls=%fused_computation | convolution fusion | flops 1882521600 | bytes 11141120 | tf_op jit(solution)/shard_map/dot_general | solution.py:144
  140.2 55.4 %all_to_all.45 = bf16[16,64,2048]{2,1,0:T(8,128)(2,1)} all-to-all(bf16[16,64,2048]{2,1,0:T(8,128)(2,1)} %bitcast.35), channel_id=1, replica_groups=mesh['sp_0'=16,'sp_1'=2,'tp'=16] {'tp'}, dimensions={0} | all-to-all | bytes 8388608 | tf_op jit(solution)/shard_map/all_to_all | solution.py:27
  195.6 3.0 %reduce_sum.45 = bf16[64,2048]{1,0:T(8,128)(2,1)S(1)} reduce(bf16[16,64,2048]{2,1,0:T(8,128)(2,1)} %all_to_all.45, bf16[]{:T(256)} %constant.97.clone.1), dimensions={0}, to_apply=%region_4.5 | reduce | flops 1966080 | bytes 4456450 | tf_op jit(solution)/shard_map/reduce_sum | solution.py:28
  199.0 3.9 %all_to_all.46 = bf16[16,2,1,2,2048]{4,3,0,2,1:T(2,128)(2,1)S(1)} all-to-all(bf16[16,2,1,2,2048]{4,3,0,2,1:T(2,128)(2,1)S(1)} %copy.20), channel_id=1, replica_groups=mesh['sp_0'=16,'sp_1'=2,'tp'=16] {'sp_1'}, dimensions={1} | all-to-all | bytes 524288 | tf_op jit(solution)/shard_map/all_to_all | solution.py:41
  202.9 1.0 copy.21
  203.9 6.8 %all-to-all-start.5 = ((bf16[16,2,1,2,2048]{4,3,1,2,0:T(2,128)(2,1)}), bf16[16,2,1,2,2048]{4,3,1,2,0:T(2,128)(2,1)S(1)}, u32[]{:S(2)}, u32[]{:S(2)}) async-start(bf16[16,2,1,2,2048]{4,3,1,2,0:T(2,128)(2,1)} %copy.21), calls=%async_computation.5 | async-start | bytes 524288 | tf_op jit(solution)/shard_map/all_to_all | solution.py:41
  210.7 0.8 dynamic-slice_bitcast_fusion
  211.8 17.2 %all-to-all-done.5 = bf16[16,2,1,2,2048]{4,3,1,2,0:T(2,128)(2,1)S(1)} async-done(((bf16[16,2,1,2,2048]{4,3,1,2,0:T(2,128)(2,1)}), bf16[16,2,1,2,2048]{4,3,1,2,0:T(2,128)(2,1)S(1)}, u32[]{:S(2)}, u32[]{:S(2)}) %all-to-all-start.5) | async-done | bytes 262176 | tf_op jit(solution)/shard_map/all_to_all | solution.py:41
  229.1 0.2 fusion
  229.5 19.4 %all_to_all.47 = bf16[16,16,2048]{2,1,0:T(8,128)(2,1)S(1)} all-to-all(bf16[16,16,2048]{2,1,0:T(8,128)(2,1)S(1)} %broadcast_in_dim.39), channel_id=1, replica_groups=mesh['sp_0'=16,'sp_1'=2,'tp'=16] {'tp'}, dimensions={0} | all-to-all | bytes 2097152 | tf_op jit(solution)/shard_map/all_to_all | solution.py:53
  248.9 1.0 copy.44
  (56 shorter events, 5.6 us)
Async XLA Ops:
  0.0 133.2 %copy-start = (bf16[1,224,2048]{2,1,0:T(8,128)(2,1)S(1)}, bf16[1,224,2048]{2,1,0:T(8,128)(2,1)}, u32[]{:S(2)}) copy-start(bf16[1,224,2048]{2,1,0:T(8,128)(2,1)} %param.19) | copy-start | bytes 2752516
  0.0 6.0 %copy-start.2 = (s32[256,2]{0,1:T(2,128)S(1)}, s32[256,2]{0,1:T(2,128)}, u32[]{:S(2)}) copy-start(s32[256,2]{0,1:T(2,128)} %param.15) | copy-start | bytes 6148
  0.0 9.1 %copy-start.6 = (f32[128]{0:T(128)S(1)}, f32[128]{0:T(128)}, u32[]{:S(2)}) copy-start(f32[128]{0:T(128)} %param.13) | copy-start | bytes 1540
  0.0 9.1 %copy-start.5 = (bf16[512,128]{1,0:T(8,128)(2,1)S(1)}, bf16[512,128]{1,0:T(8,128)(2,1)}, u32[]{:S(2)}) copy-start(bf16[512,128]{1,0:T(8,128)(2,1)} %param.12) | copy-start | bytes 393220
  4.0 5.1 %collective-permute-start = (bf16[16,512]{1,0:T(8,128)(2,1)S(1)}, bf16[16,512]{1,0:T(8,128)(2,1)S(1)}, u32[]{:S(2)}, u32[]{:S(2)}) collective-permute-start(bf16[16,512]{1,0:T(8,128)(2,1)S(1)} %slice.69), channel_id=1, source_target_pairs={{0,16},{16,32},{32,48},{48,64},{64,80},{80,96},{96,112},{112,128},... | collective-permute-start | bytes 49160 | tf_op jit(solution)/shard_map/ppermute | solution.py:17
  9.2 16.9 %copy-start.1 = (f32[2048]{0:T(1024)S(1)}, f32[2048]{0:T(1024)}, u32[]{:S(2)}) copy-start(f32[2048]{0:T(1024)} %param.14) | copy-start | bytes 24580
  11.2 14.7 %all-to-all-start = ((bf16[16,16,128]{2,1,0:T(8,128)(2,1)}), bf16[16,16,128]{2,1,0:T(8,128)(2,1)S(1)}, u32[]{:S(2)}, u32[]{:S(2)}) async-start(bf16[16,16,128]{2,1,0:T(8,128)(2,1)} %bitcast), calls=%async_computation | async-start | bytes 131072 | tf_op jit(solution)/shard_map/all_to_all | solution.py:119
  121.3 7.3 %copy-start.3 = (bf16[1,2048,224]{1,2,0:T(8,128)(2,1)S(1)}, bf16[1,2048,224]{1,2,0:T(8,128)(2,1)}, u32[]{:S(2)}) copy-start(bf16[1,2048,224]{1,2,0:T(8,128)(2,1)} %param.17) | copy-start | bytes 2752516
  128.6 4.6 %copy-start.4 = (bf16[1,2048,224]{1,2,0:T(8,128)(2,1)S(1)}, bf16[1,2048,224]{1,2,0:T(8,128)(2,1)}, u32[]{:S(2)}) copy-start(bf16[1,2048,224]{1,2,0:T(8,128)(2,1)} %param.18) | copy-start | bytes 2752516
  203.9 25.1 %all-to-all-start.5 = ((bf16[16,2,1,2,2048]{4,3,1,2,0:T(2,128)(2,1)}), bf16[16,2,1,2,2048]{4,3,1,2,0:T(2,128)(2,1)S(1)}, u32[]{:S(2)}, u32[]{:S(2)}) async-start(bf16[16,2,1,2,2048]{4,3,1,2,0:T(2,128)(2,1)} %copy.21), calls=%async_computation.5 | async-start | bytes 524288 | tf_op jit(solution)/shard_map/all_to_all | solution.py:41
